TPU v7x, 512 devices: a whole 4x4x16 slice. The times are simulated.
512 devices in a mesh: sp: 32 (over z, core), tp: 16 (over y, x).
Axes of the slice: x: 4, y: 4, z: 16, core: 2. Of those that a mesh axis runs over, the one named last changes fastest.
Arguments:
- query_a: bfloat16 [6144, 2048], P('sp', 'tp'), may hold values from -6 to 6
- key_a: bfloat16 [6144, 2048], P('sp', 'tp'), may hold values from -6 to 6
- value_a: bfloat16 [6144, 2048], P('sp', 'tp'), may hold values from -6 to 6
- query_b: bfloat16 [6144, 2048], P('sp', 'tp'), may hold values from -6 to 6
- key_b: bfloat16 [6144, 2048], P('sp', 'tp'), may hold values from -6 to 6
- value_b: bfloat16 [6144, 2048], P('sp', 'tp'), may hold values from -6 to 6
- stop_a: float32 [6144, 32], P('sp', 'tp'), may hold values from -14 to -1
- stop_b: float32 [6144, 16], P('sp', 'tp'), may hold values from -14 to -1
- out_a: bfloat16 [2048, 2048], P('tp'), may hold values from -4 to 4
- out_b: bfloat16 [2048, 2048], P('tp'), may hold values from -4 to 4
- resid: bfloat16 [6144, 2048], P('sp', 'tp'), may hold values from -20 to 20
- mix_gain: float32 [2048], P('tp'), may hold values from 0.1 to 1.9
- ffn_gain: float32 [2048], P('tp'), may hold values from 0.1 to 1.9
- routes: int32 [6144, 2], P('sp'), may hold values from 0 to 127, all different within a row; in each aligned block of 192 rows (0 to 191, 192 to 383, ...) at most 5 rows name the same one
- gates: float32 [6144, 2], P('sp'), may hold values from 0.25 to 1.5
- exp_gate: bfloat16 [128, 2048, 512], P('sp', 'tp'), may hold values from -0.125 to 0.125
- exp_up: bfloat16 [128, 2048, 512], P('sp', 'tp'), may hold values from -0.125 to 0.125
- exp_down: bfloat16 [128, 512, 2048], P('sp', None, 'tp'), may hold values from -0.25 to 0.25
- sh_gate: bfloat16 [2048, 512], P('tp'), may hold values from -0.125 to 0.125
- sh_up: bfloat16 [2048, 512], P('tp'), may hold values from -0.125 to 0.125
- sh_down: bfloat16 [512, 2048], P(None, 'tp'), may hold values from -4 to 4
Outputs:
- result: bfloat16 [6144, 2048], P('sp', 'tp')
Inputs may be any that keep to these rules, and one draw needn't show every extreme that they name: `routes`: each row names 2 different experts. Within the rows of one index of sp (aligned blocks of 192 rows) no expert is named by more than 5 rows, a bound that some block reaches.
All inputs are finite; a program needn't handle non-finite values.
Results may differ from a plain program's by a relative error of at most 0.02.
Values may be sent and summed in bfloat16 or wider, within the bound.
A program may use at most 64 MiB of HBM per device.

v0:
```python
import jax
import jax.numpy as jnp
from jax import lax
from jax.sharding import Mesh
from jax.sharding import PartitionSpec as P

D = 2048
TP = ("tp_0", "tp_1")
epsilon = 1e-06


def cut_along(x, dim, size):
    before, after = (x.shape[:dim], x.shape[dim + 1 :])
    return jnp.moveaxis(x.reshape(*before, size, -1, *after), dim, 0)


def sum_at_owner(x, axis, dim):
    tiles = cut_along(x, dim, lax.axis_size(axis))
    arrived = lax.all_to_all(tiles, axis, split_axis=0, concat_axis=0, tiled=True)
    return arrived.astype(jnp.float32).sum(axis=0)


def by_axis(x, axes):
    for axis in axes:
        x = lax.psum(x, axis)
    return x


def suffix_sums(failing):
    width = failing.shape[-1]
    pieces = width // width
    shaped = failing.reshape(failing.shape[:-1] + (pieces, width))
    places = jnp.arange(width)
    upper = (places[:, None] > places[None, :]).astype(jnp.float32)
    inner = jnp.matmul(shaped, upper)
    return inner.reshape(failing.shape)


def stick_block(state, queries, keyset, causal):
    outputs, carried = state
    new_out = []
    new_carry = []
    for group in range(2):
        query, stop, scale = queries[group]
        keys = keyset[2 * group]
        values = keyset[2 * group + 1]
        scores = jnp.einsum("qhd,khd->hqk", query, keys, preferred_element_type=jnp.float32)
        scores = scores * scale + jnp.transpose(stop)[:, :, None]
        failing = jax.nn.log_sigmoid(-scores)
        if causal is not None:
            failing = jnp.where(causal, failing, 0.0)
        after = suffix_sums(failing) + carried[group][:, :, None]
        weight = jnp.exp(jax.nn.log_sigmoid(scores) + after)
        if causal is not None:
            weight = jnp.where(causal, weight, 0.0)
        added = jnp.einsum(
            "hqk,khe->qhe", weight.astype(jnp.bfloat16), values, preferred_element_type=jnp.float32
        )
        new_out.append(outputs[group] + added)
        new_carry.append(carried[group] + jnp.sum(failing, axis=-1))
    return (tuple(new_out), tuple(new_carry))


def empty_state(count, heads_a, size_a, heads_b, size_b):
    return (
        (
            jnp.zeros((count, heads_a, size_a), jnp.float32),
            jnp.zeros((count, heads_b, size_b), jnp.float32),
        ),
        (jnp.zeros((heads_a, count), jnp.float32), jnp.zeros((heads_b, count), jnp.float32)),
    )


def joined_rows(state, width_a, width_b):
    count = state[0][0].shape[0]
    return jnp.concatenate(
        [
            state[0][0].astype(jnp.bfloat16).reshape(count, width_a),
            state[0][1].astype(jnp.bfloat16).reshape(count, width_b),
        ],
        axis=1,
    )


def shards(
    query_a,
    key_a,
    value_a,
    query_b,
    key_b,
    value_b,
    stop_a,
    stop_b,
    out_a,
    out_b,
    resid,
    mix_gain,
    ffn_gain,
    routes,
    gates,
    exp_gate,
    exp_up,
    exp_down,
    sh_gate,
    sh_up,
    sh_down,
):
    rows = query_a.shape[0]
    heads_a = stop_a.shape[1]
    heads_b = stop_b.shape[1]
    width_a = query_a.shape[1]
    width_b = query_b.shape[1]
    size_a = width_a // heads_a
    size_b = width_b // heads_b

    def unpack(joined):
        count = joined.shape[0]
        return (
            joined[:, :width_a].reshape(count, heads_a, size_a),
            joined[:, width_a : 2 * width_a].reshape(count, heads_a, size_a),
            joined[:, 2 * width_a : 2 * width_a + width_b].reshape(count, heads_b, size_b),
            joined[:, 2 * width_a + width_b :].reshape(count, heads_b, size_b),
        )

    joined_local = jnp.concatenate([key_a, value_a, key_b, value_b], axis=1)
    places = jnp.arange(rows)
    position = lax.axis_index("sp")
    n_sp = lax.axis_size("sp")
    count = query_a.shape[0]
    queries = (
        (query_a.reshape(count, heads_a, size_a), stop_a, size_a ** (-0.5)),
        (query_b.reshape(count, heads_b, size_b), stop_b, size_b ** (-0.5)),
    )
    causal = (places[None, :] < places[:, None])[None]
    state = stick_block(
        empty_state(rows, heads_a, size_a, heads_b, size_b), queries, unpack(joined_local), causal
    )
    gathered = lax.all_gather(joined_local, "sp", axis=0, tiled=True)

    def turn(step, inner_state):
        start = jnp.maximum(position - step, 0) * rows
        piece = lax.dynamic_slice_in_dim(gathered, start, rows, 0)
        return lax.cond(
            position >= step,
            lambda inputs: stick_block(inputs, queries, unpack(piece), None),
            lambda inputs: inputs,
            inner_state,
        )

    state = lax.fori_loop(1, n_sp, turn, state)
    attended = joined_rows(state, width_a, width_b)
    attended_a = attended[:, :width_a]
    attended_b = attended[:, width_a:]
    partial_value = jnp.dot(attended_a, out_a, preferred_element_type=jnp.float32)
    partial_value = partial_value + jnp.dot(attended_b, out_b, preferred_element_type=jnp.float32)
    mixed = sum_at_owner(partial_value.astype(jnp.bfloat16), TP, 1)
    mix_total = by_axis(jnp.sum(mixed * mixed, axis=1), TP)
    branch = mixed * lax.rsqrt(mix_total / D + epsilon)[:, None] * mix_gain[None, :]
    stream = lax.optimization_barrier((resid.astype(jnp.float32) + branch).astype(jnp.bfloat16))
    stream_f = stream.astype(jnp.float32)
    ffn_total = by_axis(jnp.sum(stream_f * stream_f, axis=1), TP)
    normed = (stream_f * lax.rsqrt(ffn_total / D + epsilon)[:, None] * ffn_gain[None, :]).astype(
        jnp.bfloat16
    )
    shared_gate, shared_up = (
        lax.psum(
            jnp.dot(normed, sh_gate, preferred_element_type=jnp.float32).astype(jnp.bfloat16), TP
        ).astype(jnp.float32),
        lax.psum(
            jnp.dot(normed, sh_up, preferred_element_type=jnp.float32).astype(jnp.bfloat16), TP
        ).astype(jnp.float32),
    )
    shared_hidden = (jax.nn.silu(shared_gate) * shared_up).astype(jnp.bfloat16)
    shared_out = jnp.dot(shared_hidden, sh_down, preferred_element_type=jnp.float32)
    local_experts = exp_gate.shape[0]
    experts = local_experts * n_sp
    top_count = routes.shape[1]
    capacity = max(1, (3 * rows * top_count + 2 * experts - 1) // (2 * experts))
    flat_routes = routes.reshape(-1)
    onehot = (flat_routes[:, None] == jnp.arange(experts, dtype=jnp.int32)[None, :]).astype(
        jnp.int32
    )
    earlier = jnp.cumsum(onehot, axis=0) - onehot
    slot = flat_routes * capacity + jnp.sum(earlier * onehot, axis=1)
    chooser = (slot[:, None] == jnp.arange(experts * capacity, dtype=jnp.int32)[None, :]).astype(
        jnp.bfloat16
    )
    chooser = jnp.sum(chooser.reshape(rows, top_count, experts * capacity), axis=1)
    outgoing = jnp.einsum("rs,rc->sc", chooser, normed, preferred_element_type=jnp.float32).astype(
        jnp.bfloat16
    )
    outgoing = outgoing.reshape(n_sp, local_experts, capacity, normed.shape[1])
    arrived = lax.all_to_all(outgoing, "sp", split_axis=0, concat_axis=0, tiled=True)
    gate_part = jnp.einsum("segd,edf->segf", arrived, exp_gate, preferred_element_type=jnp.float32)
    up_part = jnp.einsum("segd,edf->segf", arrived, exp_up, preferred_element_type=jnp.float32)
    gate_pre = lax.psum(gate_part.astype(jnp.bfloat16), TP).astype(jnp.float32)
    up_pre = lax.psum(up_part.astype(jnp.bfloat16), TP).astype(jnp.float32)
    hidden = (jax.nn.silu(gate_pre) * up_pre).astype(jnp.bfloat16)
    produced = jnp.einsum("segf,efd->segd", hidden, exp_down, preferred_element_type=jnp.float32)
    returned = lax.all_to_all(
        produced.astype(jnp.bfloat16), "sp", split_axis=0, concat_axis=0, tiled=True
    )
    flat_back = returned.reshape(experts * capacity, returned.shape[3])
    picked = jnp.take(flat_back, slot, axis=0).reshape(rows, top_count, returned.shape[3])
    routed = jnp.sum(gates[:, :, None] * picked.astype(jnp.float32), axis=1)
    moe = routed + shared_out
    result = stream_f + moe
    return result.astype(jnp.bfloat16)


def solution(mesh):
    finer = Mesh(mesh.devices.reshape(mesh.shape["sp"], 4, 4), ("sp", "tp_0", "tp_1"))
    in_specs = (
        P("sp", TP),
        P("sp", TP),
        P("sp", TP),
        P("sp", TP),
        P("sp", TP),
        P("sp", TP),
        P("sp", TP),
        P("sp", TP),
        P(TP, None),
        P(TP, None),
        P("sp", TP),
        P(TP),
        P(TP),
        P("sp", None),
        P("sp", None),
        P("sp", TP, None),
        P("sp", TP, None),
        P("sp", None, TP),
        P(TP, None),
        P(TP, None),
        P(None, TP),
    )
    out_specs = P("sp", TP)
    return jax.shard_map(
        shards, mesh=finer, in_specs=in_specs, out_specs=out_specs, check_vma=False
    )
```

profile of v0, /device:TPU:1, one launch (start us, length us, event | category | flops | bytes accessed | tf_op | source)
XLA Modules:
  0.0 487.4 jit_solution(6028487693172046048)
XLA Ops:
  6.5 1.6 pad_maximum_fusion
  8.2 0.9 copy.128
  9.1 0.9 copy.131
  10.0 0.9 copy.127
  10.9 0.8 copy.137
  12.0 1.1 fusion.127
  13.2 0.5 fusion.75
  13.7 0.3 fusion.133
  14.0 0.3 fusion.98
  14.3 0.2 fusion.99
  14.5 0.8 fusion.73
  15.3 76.1 %all-gather.2.cloned.1.call-done = bf16[6144,512]{1,0:T(8,128)(2,1)} async-done(((bf16[192,512]{1,0:T(8,128)(2,1)}), bf16[6144,512]{1,0:T(8,128)(2,1)}) %all-gather.2.cloned.1.call-update) | async-done | bytes 6291472 | tf_op jit(solution)/shard_map/all_gather | solution.py:138
  91.4 8.7 %copy.134 = bf16[6144,512]{0,1:T(8,128)(2,1)} copy(bf16[6144,512]{1,0:T(8,128)(2,1)} %all-gather.2.cloned.1.call-done) | data formatting | bytes 12582912 | tf_op jit(solution)/shard_map/while | solution.py:150
  100.1 6.4 %while.19 = (s32[]{:T(128)}, f32[192,2,64]{0,2,1:T(8,128)S(1)}, f32[192,1,128]{2,0,1:T(8,128)S(1)}, f32[2,192]{1,0:T(2,128)S(1)}, f32[1,192]{1,0:T(1,128)S(1)}, ...) while((s32[]{:T(128)}, f32[192,2,64]{0,2,1:T(8,128)S(1)}, ...), condition=%wide.region_7.8_spmd, body=%wide.region_2.7_spmd.sunk | while | flops 83325512 | bytes 2064037 | solution.py:150
  100.1 5.1 %conditional.2 = ((f32[192,2,64]{0,2,1:T(8,128)S(1)}, f32[192,1,128]{2,0,1:T(8,128)S(1)}, f32[2,192]{1,0:T(2,128)S(1)}, f32[1,192]{1,0:T(1,128)S(1)})) conditional(s32[]{:T(128)} %convert_element_type.258, (f32[192,2,64]{0,2,1:T(8,128)S(1)}, f32[192,1,128]{2,0,1:T(8,128)S(1)}, f32[2,192]{1,0:T(2,128)S(1)}, f32[1,192]{1,0:T(1,128)S(1)}) %tuple.58, ...), branch_computations={%region_3.3_spmd, %region_4.6_spmd} | conditional | flops 83325512 | bytes 2063786 | solution.py:143
  100.1 1.1 constant_dynamic-slice_fusion
  101.1 0.5 fusion.25
  101.6 0.7 fusion.12
  102.4 1.3 fusion.43
  103.7 1.5 fusion.13
  106.5 0.4 fusion.154
  106.9 0.6 copy-done.1
  107.5 0.4 fusion.60
  107.9 1.1 copy.166
  109.0 6.7 %all-to-all-start = ((bf16[16,192,128]{2,1,0:T(8,128)(2,1)}), bf16[16,192,128]{2,1,0:T(8,128)(2,1)S(1)}, u32[]{:S(2)}, u32[]{:S(2)}) async-start(bf16[16,192,128]{2,1,0:T(8,128)(2,1)} %bitcast.107), calls=%async_computation | async-start | bytes 1572864 | tf_op jit(solution)/shard_map/all_to_all | solution.py:19
  116.0 0.2 fusion.108
  116.6 9.7 %all-to-all-done = bf16[16,192,128]{2,1,0:T(8,128)(2,1)S(1)} async-done(((bf16[16,192,128]{2,1,0:T(8,128)(2,1)}), bf16[16,192,128]{2,1,0:T(8,128)(2,1)S(1)}, u32[]{:S(2)}, u32[]{:S(2)}) %all-to-all-start) | async-done | bytes 786464 | tf_op jit(solution)/shard_map/all_to_all | solution.py:19
  126.6 6.5 %psum.56 = f32[192]{0:T(256)S(1)} all-reduce(f32[192]{0:T(256)S(1)} %multiply_reduce_fusion.1), channel_id=1, replica_groups=mesh['sp'=32,'tp_0'=4,'tp_1'=4] {'tp_0'}, use_global_device_ids=true, to_apply=%region_10.11 | all-reduce | flops 192 | bytes 1536 | tf_op jit(solution)/shard_map/psum | solution.py:25
  133.1 6.8 %psum.57 = f32[192]{0:T(256)S(1)} all-reduce(f32[192]{0:T(256)S(1)} %psum.56), channel_id=1, replica_groups=mesh['sp'=32,'tp_0'=4,'tp_1'=4] {'tp_1'}, use_global_device_ids=true, to_apply=%region_11.12 | all-reduce | flops 192 | bytes 1536 | tf_op jit(solution)/shard_map/psum | solution.py:25
  140.1 6.5 %psum.58 = f32[192]{0:T(256)S(1)} all-reduce(f32[192]{0:T(256)S(1)} %fusion.130), channel_id=1, replica_groups=mesh['sp'=32,'tp_0'=4,'tp_1'=4] {'tp_0'}, use_global_device_ids=true, to_apply=%region_17.18 | all-reduce | flops 192 | bytes 1536 | tf_op jit(solution)/shard_map/psum | solution.py:25
  146.6 7.1 %psum.59 = f32[192]{0:T(256)S(1)} all-reduce(f32[192]{0:T(256)S(1)} %psum.58), channel_id=1, replica_groups=mesh['sp'=32,'tp_0'=4,'tp_1'=4] {'tp_1'}, use_global_device_ids=true, to_apply=%region_18.19 | all-reduce | flops 192 | bytes 1536 | tf_op jit(solution)/shard_map/psum | solution.py:25
  153.7 0.3 convolution_convert_fusion.5
  154.1 0.7 copy.143
  154.9 161.9 %all-to-all-start.1 = ((bf16[32,4,5,128]{3,1,2,0:T(4,128)(2,1)}), bf16[32,4,5,128]{3,1,2,0:T(4,128)(2,1)S(1)}, u32[]{:S(2)}, u32[]{:S(2)}) async-start(bf16[32,4,5,128]{3,1,2,0:T(4,128)(2,1)} %copy.143), calls=%async_computation.1 | async-start | bytes 327680 | tf_op jit(solution)/shard_map/all_to_all | solution.py:193
  316.8 0.9 convolution_convert_fusion.3
  317.7 0.9 convolution_convert_fusion.2
  318.7 15.2 %all-to-all-done.1 = bf16[32,4,5,128]{3,1,2,0:T(4,128)(2,1)S(1)} async-done(((bf16[32,4,5,128]{3,1,2,0:T(4,128)(2,1)}), bf16[32,4,5,128]{3,1,2,0:T(4,128)(2,1)S(1)}, u32[]{:S(2)}, u32[]{:S(2)}) %all-to-all-start.1) | async-done | bytes 163872 | tf_op jit(solution)/shard_map/all_to_all | solution.py:193
  333.9 1.2 fusion.61
  335.0 1.2 fusion.62
  336.2 106.3 %all-reduce.3.cloned.1.call-done = (bf16[32,4,5,512]{3,0,2,1:T(8,128)(2,1)}, bf16[32,4,5,512]{3,0,2,1:T(8,128)(2,1)}, bf16[192,512]{1,0:T(8,128)(2,1)}, bf16[192,512]{1,0:T(8,128)(2,1)}) async-done(((bf16[32,4,5,512]{3,0,2,1:T(8,128)(2,1)}, bf16[32,4,5,512]{3,0,2,1:T(8,128)(2,1)}, bf16[192,512]{1,0:T(8,128)(2,1)}, bf16[192,512]{1,0:T(8,128)(2,1)}), (bf16[32,4,5,512]{3,0,2,1:T(8,128)(2,1)}, ...) | async-done | bytes 1703952 | tf_op jit(solution)/shard_map/psum | solution.py:197
  442.6 1.8 fusion.71
  444.5 0.7 copy.146
  445.2 14.6 %all-to-all-start.2 = ((bf16[32,4,5,128]{3,1,2,0:T(4,128)(2,1)}), bf16[32,4,5,128]{3,1,2,0:T(4,128)(2,1)S(1)}, u32[]{:S(2)}, u32[]{:S(2)}) async-start(bf16[32,4,5,128]{3,1,2,0:T(4,128)(2,1)} %copy.146), calls=%async_computation.2 | async-start | bytes 327680 | tf_op jit(solution)/shard_map/all_to_all | solution.py:200
  460.1 0.2 copy.142
  460.5 16.5 %all-to-all-done.2 = bf16[32,4,5,128]{3,1,2,0:T(4,128)(2,1)S(1)} async-done(((bf16[32,4,5,128]{3,1,2,0:T(4,128)(2,1)}), bf16[32,4,5,128]{3,1,2,0:T(4,128)(2,1)S(1)}, u32[]{:S(2)}, u32[]{:S(2)}) %all-to-all-start.2) | async-done | bytes 163872 | tf_op jit(solution)/shard_map/all_to_all | solution.py:200
  477.1 1.4 gather_fusion
  478.6 1.1 multiply_reduce_fusion
  479.7 0.9 fusion.77
  (102 shorter events, 2.6 us)
Async XLA Ops:
  6.5 100.0 %copy-start = (bf16[128,2048]{1,0:T(8,128)(2,1)S(1)}, bf16[128,2048]{1,0:T(8,128)(2,1)}, u32[]{:S(2)}) copy-start(bf16[128,2048]{1,0:T(8,128)(2,1)} %param.33) | copy-start | bytes 1572868
  6.5 6.6 %copy-start.6 = (bf16[192,128]{1,0:T(8,128)(2,1)S(1)}, bf16[192,128]{1,0:T(8,128)(2,1)}, u32[]{:S(2)}) copy-start(bf16[192,128]{1,0:T(8,128)(2,1)} %param.30) | copy-start | bytes 147460
  6.5 84.8 %all-gather.2.cloned.1.call-start = ((), (), s32[]{:S(2)}) async-start(), calls=%async_computation.3 | async-start | bytes 6488064 | tf_op jit(solution)/shard_map/all_gather | solution.py:138
  8.2 5.5 %copy-start.10 = (f32[192,2]{0,1:T(2,128)S(1)}, f32[192,2]{0,1:T(2,128)}, u32[]{:S(2)}) copy-start(f32[192,2]{0,1:T(2,128)} %param.31) | copy-start | bytes 4612
  15.2 84.8 %copy-start.17 = (bf16[192,128]{1,0:T(8,128)(2,1)S(1)}, bf16[192,128]{1,0:T(8,128)(2,1)}, u32[]{:S(2)}) copy-start(bf16[192,128]{1,0:T(8,128)(2,1)} %param.28) | copy-start | bytes 147460
  15.3 84.8 %copy-start.18 = (f32[192,1]{0,1:T(1,128)S(1)}, f32[192,1]{0,1:T(1,128)}, u32[]{:S(2)}) copy-start(f32[192,1]{0,1:T(1,128)} %param.32) | copy-start | bytes 2308
  106.5 1.0 copy-start.1
  109.0 7.4 %copy-start.8 = (s32[192,2]{0,1:T(2,128)S(1)}, s32[192,2]{0,1:T(2,128)}, u32[]{:S(2)}) copy-start(s32[192,2]{0,1:T(2,128)} %param.38) | copy-start | bytes 4612
  109.0 17.3 %all-to-all-start = ((bf16[16,192,128]{2,1,0:T(8,128)(2,1)}), bf16[16,192,128]{2,1,0:T(8,128)(2,1)S(1)}, u32[]{:S(2)}, u32[]{:S(2)}) async-start(bf16[16,192,128]{2,1,0:T(8,128)(2,1)} %bitcast.107), calls=%async_computation | async-start | bytes 1572864 | tf_op jit(solution)/shard_map/all_to_all | solution.py:19
  115.7 24.2 %copy-start.7 = (bf16[192,128]{1,0:T(8,128)(2,1)S(1)}, bf16[192,128]{1,0:T(8,128)(2,1)}, u32[]{:S(2)}) copy-start(bf16[192,128]{1,0:T(8,128)(2,1)} %param.35) | copy-start | bytes 147460
  115.7 24.2 %copy-start.12 = (f32[128]{0:T(128)S(1)}, f32[128]{0:T(128)}, u32[]{:S(2)}) copy-start(f32[128]{0:T(128)} %param.36) | copy-start | bytes 1540
  115.7 38.0 %copy-start.9 = (f32[128]{0:T(128)S(1)}, f32[128]{0:T(128)}, u32[]{:S(2)}) copy-start(f32[128]{0:T(128)} %param.37) | copy-start | bytes 1540
  116.4 200.3 %copy-start.4 = (bf16[128,512]{1,0:T(8,128)(2,1)S(1)}, bf16[128,512]{1,0:T(8,128)(2,1)}, u32[]{:S(2)}) copy-start(bf16[128,512]{1,0:T(8,128)(2,1)} %param.43) | copy-start | bytes 393220
  116.6 201.1 %copy-start.5 = (bf16[128,512]{1,0:T(8,128)(2,1)S(1)}, bf16[128,512]{1,0:T(8,128)(2,1)}, u32[]{:S(2)}) copy-start(bf16[128,512]{1,0:T(8,128)(2,1)} %param.44) | copy-start | bytes 393220
  126.4 207.4 %copy-start.2 = (bf16[4,128,512]{2,1,0:T(8,128)(2,1)S(1)}, bf16[4,128,512]{2,1,0:T(8,128)(2,1)}, u32[]{:S(2)}) copy-start(bf16[4,128,512]{2,1,0:T(8,128)(2,1)} %param.40) | copy-start | bytes 1572868
  154.0 181.0 %copy-start.3 = (bf16[4,128,512]{2,1,0:T(8,128)(2,1)S(1)}, bf16[4,128,512]{2,1,0:T(8,128)(2,1)}, u32[]{:S(2)}) copy-start(bf16[4,128,512]{2,1,0:T(8,128)(2,1)} %param.41) | copy-start | bytes 1572868
  154.9 179.0 %all-to-all-start.1 = ((bf16[32,4,5,128]{3,1,2,0:T(4,128)(2,1)}), bf16[32,4,5,128]{3,1,2,0:T(4,128)(2,1)S(1)}, u32[]{:S(2)}, u32[]{:S(2)}) async-start(bf16[32,4,5,128]{3,1,2,0:T(4,128)(2,1)} %copy.143), calls=%async_computation.1 | async-start | bytes 327680 | tf_op jit(solution)/shard_map/all_to_all | solution.py:193
  316.7 125.9 %all-reduce.3.cloned.1.call-start = ((), (), s32[]{:S(2)}) async-start(), calls=%async_computation.4 | async-start | bytes 3407872 | tf_op jit(solution)/shard_map/psum | solution.py:197
  335.0 107.6 %copy-start.13 = (bf16[4,512,128]{2,1,0:T(8,128)(2,1)S(1)}, bf16[4,512,128]{2,1,0:T(8,128)(2,1)}, u32[]{:S(2)}) copy-start(bf16[4,512,128]{2,1,0:T(8,128)(2,1)} %param.42) | copy-start | bytes 1572868
  442.6 17.7 %copy-start.11 = (f32[192,2]{0,1:T(2,128)S(1)}, f32[192,2]{0,1:T(2,128)}, u32[]{:S(2)}) copy-start(f32[192,2]{0,1:T(2,128)} %param.39) | copy-start | bytes 4612
  444.4 35.2 %copy-start.14 = (bf16[192,512]{1,0:T(8,128)(2,1)S(1)}, bf16[192,512]{1,0:T(8,128)(2,1)}, u32[]{:S(2)}) copy-start(bf16[192,512]{1,0:T(8,128)(2,1)} %get-tuple-element.401) | copy-start | bytes 589828
  444.5 35.2 %copy-start.15 = (bf16[192,512]{1,0:T(8,128)(2,1)S(1)}, bf16[192,512]{1,0:T(8,128)(2,1)}, u32[]{:S(2)}) copy-start(bf16[192,512]{1,0:T(8,128)(2,1)} %get-tuple-element.402) | copy-start | bytes 589828
  444.5 35.2 %copy-start.16 = (bf16[512,128]{1,0:T(8,128)(2,1)S(1)}, bf16[512,128]{1,0:T(8,128)(2,1)}, u32[]{:S(2)}) copy-start(bf16[512,128]{1,0:T(8,128)(2,1)} %param.45) | copy-start | bytes 393220
  445.2 31.7 %all-to-all-start.2 = ((bf16[32,4,5,128]{3,1,2,0:T(4,128)(2,1)}), bf16[32,4,5,128]{3,1,2,0:T(4,128)(2,1)S(1)}, u32[]{:S(2)}, u32[]{:S(2)}) async-start(bf16[32,4,5,128]{3,1,2,0:T(4,128)(2,1)} %copy.146), calls=%async_computation.2 | async-start | bytes 327680 | tf_op jit(solution)/shard_map/all_to_all | solution.py:200
Sparse Core Ops, SparseCore 0:
  9.5 81.8 all-gather.1
  336.4 106.1 all-reduce.2
where the time goes:
time: 491 us; the launch traced here: 487 us
  waiting for transfers between devices  224 us (46%)
  starting transfers between devices  183 us (37%)
  blocking collectives  26.9 us (5%)
  local copies, waits for them, and re-layouts  19.3 us (4%)
  matrix products  14.7 us (3%)
  between operations  13.9 us (3%)
    all_to_all x1, starting transfers between devices, shards(): lax.all_to_all(outgoing, 'sp', split_axis=0, concat_axis=0, tiled=True)  162 us
    psum x1, waiting for transfers between devices, shards(): up_pre = lax.psum(up_part.astype(jnp.bfloat16), TP).astype(jnp.float32)  106 us
    all_gather x1, waiting for transfers between devices, shards(): gathered = lax.all_gather(joined_local, 'sp', axis=0, tiled=True)  76.1 us
    psum x4, blocking collectives, by_axis(): x = lax.psum(x, axis)  26.9 us
    all_to_all x1, waiting for transfers between devices, shards(): lax.all_to_all(produced.astype(jnp.bfloat16), 'sp', split_axis=0, concat_...  16.5 us
    all_to_all x1, waiting for transfers between devices, shards(): lax.all_to_all(outgoing, 'sp', split_axis=0, concat_axis=0, tiled=True)  15.2 us
    all_to_all x1, starting transfers between devices, shards(): lax.all_to_all(produced.astype(jnp.bfloat16), 'sp', split_axis=0, concat_...  14.6 us
  transfers between devices with their start and end apart: 5, of which 5 were waited for; matrix products, arithmetic and copies ran while one was open for 2% of the time, Pallas kernels for 0%

commit v1 on v0

--- a/solution.py
+++ b/solution.py
@@ -135,7 +135,9 @@
     state = stick_block(
         empty_state(rows, heads_a, size_a, heads_b, size_b), queries, unpack(joined_local), causal
     )
-    gathered = lax.all_gather(joined_local, "sp", axis=0, tiled=True)
+    gathered = jnp.concatenate(
+        lax.all_to_all(jnp.stack([joined_local] * lax.axis_size("sp")), "sp", 0, 0), axis=0
+    )
 
     def turn(step, inner_state):
         start = jnp.maximum(position - step, 0) * rows

time: 491 us -> 698 us (1.42)
  waiting for transfers between devices: 224 us -> 419 us
  starting transfers between devices: 183 us -> 196 us
    all_to_all x0 -> x1, waiting for transfers between devices: none -> 271 us  [shards(): lax.all_to_all(jnp.stack([joined_local] * lax.axis_size('sp')), 'sp', 0, 0)]
    all_gather x1 -> x0, waiting for transfers between devices: 76.1 us -> none  [shards(): gathered = lax.all_gather(joined_local, 'sp', axis=0, tiled=True)]
    all_to_all x0 -> x1, starting transfers between devices: none -> 16.9 us  [shards(): lax.all_to_all(jnp.stack([joined_local] * lax.axis_size('sp')), 'sp', 0, 0)]
  transfers between devices with their start and end apart: 5 -> 5, of which waited for: 5 -> 5; matrix products, arithmetic and copies ran while one was open for 2% -> 1% of each run, Pallas kernels for 0% -> 0%
where the time goes in v1:
time: 698 us; the launch traced here: 694 us
  waiting for transfers between devices  419 us (60%)
  starting transfers between devices  196 us (28%)
  blocking collectives  26.9 us (4%)
  local copies, waits for them, and re-layouts  19.6 us (3%)
  between operations  13.9 us (2%)
  matrix products  13.8 us (2%)
    all_to_all x1, waiting for transfers between devices, shards(): lax.all_to_all(jnp.stack([joined_local] * lax.axis_size('sp')), 'sp', 0, 0)  271 us
    all_to_all x1, starting transfers between devices, shards(): lax.all_to_all(outgoing, 'sp', split_axis=0, concat_axis=0, tiled=True)  157 us
    psum x1, waiting for transfers between devices, shards(): up_pre = lax.psum(up_part.astype(jnp.bfloat16), TP).astype(jnp.float32)  106 us
    psum x4, blocking collectives, by_axis(): x = lax.psum(x, axis)  26.9 us
    all_to_all x1, starting transfers between devices, shards(): lax.all_to_all(jnp.stack([joined_local] * lax.axis_size('sp')), 'sp', 0, 0)  16.9 us
    all_to_all x1, waiting for transfers between devices, shards(): lax.all_to_all(produced.astype(jnp.bfloat16), 'sp', split_axis=0, concat_...  16.5 us
    all_to_all x1, waiting for transfers between devices, shards(): lax.all_to_all(outgoing, 'sp', split_axis=0, concat_axis=0, tiled=True)  15.2 us
    all_to_all x1, starting transfers between devices, shards(): lax.all_to_all(produced.astype(jnp.bfloat16), 'sp', split_axis=0, concat_...  14.6 us
  transfers between devices with their start and end apart: 5, of which 5 were waited for; matrix products, arithmetic and copies ran while one was open for 1% of the time, Pallas kernels for 0%

profile of v1, /device:TPU:1, one launch (start us, length us, event | category | flops | bytes accessed | tf_op | source)
XLA Modules:
  0.0 694.3 jit_solution(3236648173123781317)
XLA Ops:
  6.5 1.0 pad_maximum_fusion
  7.5 3.4 stack.2
  10.9 16.9 %all-to-all-start = ((bf16[32,192,512]{2,1,0:T(8,128)(2,1)}), bf16[32,192,512]{2,1,0:T(8,128)(2,1)}, u32[]{:S(2)}, u32[]{:S(2)}) async-start(bf16[32,192,512]{2,1,0:T(8,128)(2,1)} %stack.2), calls=%async_computation | async-start | bytes 12582912 | tf_op jit(solution)/shard_map/all_to_all | solution.py:139
  28.7 0.3 fusion.127
  29.0 0.5 fusion.75
  29.5 0.3 fusion.133
  29.8 0.3 fusion.98
  30.1 0.2 fusion.99
  30.3 0.8 fusion.73
  31.1 271.5 %all-to-all-done = bf16[32,192,512]{2,1,0:T(8,128)(2,1)} async-done(((bf16[32,192,512]{2,1,0:T(8,128)(2,1)}), bf16[32,192,512]{2,1,0:T(8,128)(2,1)}, u32[]{:S(2)}, u32[]{:S(2)}) %all-to-all-start) | async-done | bytes 6291488 | tf_op jit(solution)/shard_map/all_to_all | solution.py:139
  302.6 8.7 %copy.128 = bf16[6144,512]{0,1:T(8,128)(2,1)} copy(bf16[6144,512]{1,0:T(8,128)(2,1)} %bitcast.24) | data formatting | bytes 12582912 | tf_op jit(solution)/shard_map/while | solution.py:152
  311.3 6.4 while.19
  311.3 5.1 conditional.2
  311.3 1.1 constant_dynamic-slice_fusion
  312.3 0.5 fusion.25
  312.8 0.7 fusion.12
  313.5 1.3 fusion.43
  314.8 1.5 fusion.13
  317.7 0.4 fusion.154
  318.1 0.6 copy-done.1
  318.7 0.4 fusion.60
  319.1 1.1 copy.160
  320.2 6.8 all-to-all-start.1
  327.2 0.2 fusion.108
  327.5 0.1 reduce_sum.108
  327.7 0.2 fusion.83
  327.9 9.7 %all-to-all-done.1 = bf16[16,192,128]{2,1,0:T(8,128)(2,1)S(1)} async-done(((bf16[16,192,128]{2,1,0:T(8,128)(2,1)}), bf16[16,192,128]{2,1,0:T(8,128)(2,1)S(1)}, u32[]{:S(2)}, u32[]{:S(2)}) %all-to-all-start.1) | async-done | bytes 786464 | tf_op jit(solution)/shard_map/all_to_all | solution.py:19
  337.8 6.5 psum.56
  344.3 6.8 psum.57
  351.3 6.5 psum.58
  357.9 7.1 %psum.59 = f32[192]{0:T(256)S(1)} all-reduce(f32[192]{0:T(256)S(1)} %psum.58), channel_id=1, replica_groups=mesh['sp'=32,'tp_0'=4,'tp_1'=4] {'tp_1'}, use_global_device_ids=true, to_apply=%region_18.19 | all-reduce | flops 192 | bytes 1536 | tf_op jit(solution)/shard_map/psum | solution.py:25
  365.0 0.3 convolution_convert_fusion.5
  365.4 0.7 copy.137
  366.1 157.5 %all-to-all-start.2 = ((bf16[32,4,5,128]{3,1,2,0:T(4,128)(2,1)}), bf16[32,4,5,128]{3,1,2,0:T(4,128)(2,1)S(1)}, u32[]{:S(2)}, u32[]{:S(2)}) async-start(bf16[32,4,5,128]{3,1,2,0:T(4,128)(2,1)} %copy.137), calls=%async_computation.2 | async-start | bytes 327680 | tf_op jit(solution)/shard_map/all_to_all | solution.py:195
  523.6 0.9 convolution_convert_fusion.3
  524.6 0.9 convolution_convert_fusion.2
  525.5 15.2 %all-to-all-done.2 = bf16[32,4,5,128]{3,1,2,0:T(4,128)(2,1)S(1)} async-done(((bf16[32,4,5,128]{3,1,2,0:T(4,128)(2,1)}), bf16[32,4,5,128]{3,1,2,0:T(4,128)(2,1)S(1)}, u32[]{:S(2)}, u32[]{:S(2)}) %all-to-all-start.2) | async-done | bytes 163872 | tf_op jit(solution)/shard_map/all_to_all | solution.py:195
  540.7 1.2 fusion.61
  541.9 1.2 fusion.62
  543.1 106.4 %all-reduce.3.cloned.1.call-done = (bf16[32,4,5,512]{3,0,2,1:T(8,128)(2,1)}, bf16[32,4,5,512]{3,0,2,1:T(8,128)(2,1)}, bf16[192,512]{1,0:T(8,128)(2,1)}, bf16[192,512]{1,0:T(8,128)(2,1)}) async-done(((bf16[32,4,5,512]{3,0,2,1:T(8,128)(2,1)}, bf16[32,4,5,512]{3,0,2,1:T(8,128)(2,1)}, bf16[192,512]{1,0:T(8,128)(2,1)}, bf16[192,512]{1,0:T(8,128)(2,1)}), (bf16[32,4,5,512]{3,0,2,1:T(8,128)(2,1)}, ...) | async-done | bytes 1703952 | tf_op jit(solution)/shard_map/psum | solution.py:199
  649.5 1.8 fusion.71
  651.4 0.7 copy.140
  652.1 14.6 %all-to-all-start.3 = ((bf16[32,4,5,128]{3,1,2,0:T(4,128)(2,1)}), bf16[32,4,5,128]{3,1,2,0:T(4,128)(2,1)S(1)}, u32[]{:S(2)}, u32[]{:S(2)}) async-start(bf16[32,4,5,128]{3,1,2,0:T(4,128)(2,1)} %copy.140), calls=%async_computation.3 | async-start | bytes 327680 | tf_op jit(solution)/shard_map/all_to_all | solution.py:202
  667.0 0.2 copy.136
  667.3 16.5 %all-to-all-done.3 = bf16[32,4,5,128]{3,1,2,0:T(4,128)(2,1)S(1)} async-done(((bf16[32,4,5,128]{3,1,2,0:T(4,128)(2,1)}), bf16[32,4,5,128]{3,1,2,0:T(4,128)(2,1)S(1)}, u32[]{:S(2)}, u32[]{:S(2)}) %all-to-all-start.3) | async-done | bytes 163872 | tf_op jit(solution)/shard_map/all_to_all | solution.py:202
  684.0 1.4 gather_fusion
  685.4 1.1 multiply_reduce_fusion
  686.6 0.9 fusion.77
  (110 shorter events, 2.7 us)
Async XLA Ops:
  6.5 311.2 %copy-start = (bf16[128,2048]{1,0:T(8,128)(2,1)S(1)}, bf16[128,2048]{1,0:T(8,128)(2,1)}, u32[]{:S(2)}) copy-start(bf16[128,2048]{1,0:T(8,128)(2,1)} %param.33) | copy-start | bytes 1572868
  10.9 17.0 %copy-start.4 = (bf16[192,128]{1,0:T(8,128)(2,1)S(1)}, bf16[192,128]{1,0:T(8,128)(2,1)}, u32[]{:S(2)}) copy-start(bf16[192,128]{1,0:T(8,128)(2,1)} %param.26) | copy-start | bytes 147460
  10.9 17.1 %copy-start.5 = (bf16[192,128]{1,0:T(8,128)(2,1)S(1)}, bf16[192,128]{1,0:T(8,128)(2,1)}, u32[]{:S(2)}) copy-start(bf16[192,128]{1,0:T(8,128)(2,1)} %param.27) | copy-start | bytes 147460
  10.9 17.3 %copy-start.8 = (bf16[192,128]{1,0:T(8,128)(2,1)S(1)}, bf16[192,128]{1,0:T(8,128)(2,1)}, u32[]{:S(2)}) copy-start(bf16[192,128]{1,0:T(8,128)(2,1)} %param.25) | copy-start | bytes 147460
  10.9 17.4 %copy-start.12 = (s32[192,2]{0,1:T(2,128)S(1)}, s32[192,2]{0,1:T(2,128)}, u32[]{:S(2)}) copy-start(s32[192,2]{0,1:T(2,128)} %param.38) | copy-start | bytes 4612
  10.9 17.8 %copy-start.9 = (bf16[192,128]{1,0:T(8,128)(2,1)S(1)}, bf16[192,128]{1,0:T(8,128)(2,1)}, u32[]{:S(2)}) copy-start(bf16[192,128]{1,0:T(8,128)(2,1)} %param.29) | copy-start | bytes 147460
  10.9 17.8 %copy-start.21 = (bf16[192,128]{1,0:T(8,128)(2,1)S(1)}, bf16[192,128]{1,0:T(8,128)(2,1)}, u32[]{:S(2)}) copy-start(bf16[192,128]{1,0:T(8,128)(2,1)} %param.28) | copy-start | bytes 147460
  10.9 17.8 %copy-start.22 = (f32[192,1]{0,1:T(1,128)S(1)}, f32[192,1]{0,1:T(1,128)}, u32[]{:S(2)}) copy-start(f32[192,1]{0,1:T(1,128)} %param.32) | copy-start | bytes 2308
  10.9 18.1 %copy-start.10 = (bf16[192,128]{1,0:T(8,128)(2,1)S(1)}, bf16[192,128]{1,0:T(8,128)(2,1)}, u32[]{:S(2)}) copy-start(bf16[192,128]{1,0:T(8,128)(2,1)} %param.30) | copy-start | bytes 147460
  10.9 291.6 %all-to-all-start = ((bf16[32,192,512]{2,1,0:T(8,128)(2,1)}), bf16[32,192,512]{2,1,0:T(8,128)(2,1)}, u32[]{:S(2)}, u32[]{:S(2)}) async-start(bf16[32,192,512]{2,1,0:T(8,128)(2,1)} %stack.2), calls=%async_computation | async-start | bytes 12582912 | tf_op jit(solution)/shard_map/all_to_all | solution.py:139
  27.9 1.6 copy-start.14
  317.7 1.0 copy-start.1
  320.2 17.4 %all-to-all-start.1 = ((bf16[16,192,128]{2,1,0:T(8,128)(2,1)}), bf16[16,192,128]{2,1,0:T(8,128)(2,1)S(1)}, u32[]{:S(2)}, u32[]{:S(2)}) async-start(bf16[16,192,128]{2,1,0:T(8,128)(2,1)} %bitcast.108), calls=%async_computation.1 | async-start | bytes 1572864 | tf_op jit(solution)/shard_map/all_to_all | solution.py:19
  326.9 24.2 %copy-start.11 = (bf16[192,128]{1,0:T(8,128)(2,1)S(1)}, bf16[192,128]{1,0:T(8,128)(2,1)}, u32[]{:S(2)}) copy-start(bf16[192,128]{1,0:T(8,128)(2,1)} %param.35) | copy-start | bytes 147460
  326.9 24.2 %copy-start.16 = (f32[128]{0:T(128)S(1)}, f32[128]{0:T(128)}, u32[]{:S(2)}) copy-start(f32[128]{0:T(128)} %param.36) | copy-start | bytes 1540
  326.9 38.0 %copy-start.13 = (f32[128]{0:T(128)S(1)}, f32[128]{0:T(128)}, u32[]{:S(2)}) copy-start(f32[128]{0:T(128)} %param.37) | copy-start | bytes 1540
  327.7 196.0 %copy-start.6 = (bf16[128,512]{1,0:T(8,128)(2,1)S(1)}, bf16[128,512]{1,0:T(8,128)(2,1)}, u32[]{:S(2)}) copy-start(bf16[128,512]{1,0:T(8,128)(2,1)} %param.43) | copy-start | bytes 393220
  327.9 196.7 %copy-start.7 = (bf16[128,512]{1,0:T(8,128)(2,1)S(1)}, bf16[128,512]{1,0:T(8,128)(2,1)}, u32[]{:S(2)}) copy-start(bf16[128,512]{1,0:T(8,128)(2,1)} %param.44) | copy-start | bytes 393220
  337.7 203.0 %copy-start.2 = (bf16[4,128,512]{2,1,0:T(8,128)(2,1)S(1)}, bf16[4,128,512]{2,1,0:T(8,128)(2,1)}, u32[]{:S(2)}) copy-start(bf16[4,128,512]{2,1,0:T(8,128)(2,1)} %param.40) | copy-start | bytes 1572868
  365.3 176.6 %copy-start.3 = (bf16[4,128,512]{2,1,0:T(8,128)(2,1)S(1)}, bf16[4,128,512]{2,1,0:T(8,128)(2,1)}, u32[]{:S(2)}) copy-start(bf16[4,128,512]{2,1,0:T(8,128)(2,1)} %param.41) | copy-start | bytes 1572868
  366.1 174.6 %all-to-all-start.2 = ((bf16[32,4,5,128]{3,1,2,0:T(4,128)(2,1)}), bf16[32,4,5,128]{3,1,2,0:T(4,128)(2,1)S(1)}, u32[]{:S(2)}, u32[]{:S(2)}) async-start(bf16[32,4,5,128]{3,1,2,0:T(4,128)(2,1)} %copy.137), calls=%async_computation.2 | async-start | bytes 327680 | tf_op jit(solution)/shard_map/all_to_all | solution.py:195
  523.6 125.9 %all-reduce.3.cloned.1.call-start = ((), (), s32[]{:S(2)}) async-start(), calls=%async_computation.4 | async-start | bytes 3407872 | tf_op jit(solution)/shard_map/psum | solution.py:199
  541.9 107.6 %copy-start.17 = (bf16[4,512,128]{2,1,0:T(8,128)(2,1)S(1)}, bf16[4,512,128]{2,1,0:T(8,128)(2,1)}, u32[]{:S(2)}) copy-start(bf16[4,512,128]{2,1,0:T(8,128)(2,1)} %param.42) | copy-start | bytes 1572868
  649.5 17.7 %copy-start.15 = (f32[192,2]{0,1:T(2,128)S(1)}, f32[192,2]{0,1:T(2,128)}, u32[]{:S(2)}) copy-start(f32[192,2]{0,1:T(2,128)} %param.39) | copy-start | bytes 4612
  651.3 35.2 %copy-start.18 = (bf16[192,512]{1,0:T(8,128)(2,1)S(1)}, bf16[192,512]{1,0:T(8,128)(2,1)}, u32[]{:S(2)}) copy-start(bf16[192,512]{1,0:T(8,128)(2,1)} %get-tuple-element.412) | copy-start | bytes 589828
  651.3 35.2 %copy-start.19 = (bf16[192,512]{1,0:T(8,128)(2,1)S(1)}, bf16[192,512]{1,0:T(8,128)(2,1)}, u32[]{:S(2)}) copy-start(bf16[192,512]{1,0:T(8,128)(2,1)} %get-tuple-element.413) | copy-start | bytes 589828
  651.4 35.2 %copy-start.20 = (bf16[512,128]{1,0:T(8,128)(2,1)S(1)}, bf16[512,128]{1,0:T(8,128)(2,1)}, u32[]{:S(2)}) copy-start(bf16[512,128]{1,0:T(8,128)(2,1)} %param.45) | copy-start | bytes 393220
  652.1 31.7 %all-to-all-start.3 = ((bf16[32,4,5,128]{3,1,2,0:T(4,128)(2,1)}), bf16[32,4,5,128]{3,1,2,0:T(4,128)(2,1)S(1)}, u32[]{:S(2)}, u32[]{:S(2)}) async-start(bf16[32,4,5,128]{3,1,2,0:T(4,128)(2,1)} %copy.140), calls=%async_computation.3 | async-start | bytes 327680 | tf_op jit(solution)/shard_map/all_to_all | solution.py:202
Sparse Core Ops, SparseCore 0:
  543.2 106.2 all-reduce.2
